TPU v7x, 128 devices: a whole 4x4x4 slice. The times are simulated.
128 devices in a mesh: sp: 16 (over z, y), tp: 8 (over x, core).
Axes of the slice: x: 4, y: 4, z: 4, core: 2. Of those that a mesh axis runs over, the one named last changes fastest.
Arguments:
- resid: bfloat16 [16384, 2048], P(('sp', 'tp')), may hold values from -6 to 6
- query_nope: bfloat16 [16384, 2048], P('sp', 'tp'), may hold values from -18 to 18
- query_rope: bfloat16 [16384, 1024], P('sp', 'tp'), may hold values from -300 to 300
- latent: bfloat16 [16384, 256], P('sp'), may hold values from -6 to 6
- key_rope: bfloat16 [16384, 64], P('sp'), may hold values from -6 to 6
- latent_gain: float32 [256], replicated, may hold values from 0.1 to 1.9
- w_key: bfloat16 [256, 2048], P(None, 'tp'), may hold values from -0.375 to 0.375
- w_value: bfloat16 [256, 2048], P(None, 'tp'), may hold values from -0.375 to 0.375
- w_out: bfloat16 [2048, 2048], P('tp'), may hold values from -0.125 to 0.125
- mix_gain: float32 [2048], replicated, may hold values from 0.1 to 1.9
- w_gate: bfloat16 [2048, 5632], P('sp', 'tp'), may hold values from -0.125 to 0.125
- w_up: bfloat16 [2048, 5632], P('sp', 'tp'), may hold values from -0.125 to 0.125
- w_down: bfloat16 [2048, 5632], P('sp', 'tp'), may hold values from -0.078125 to 0.078125
Outputs:
- layer_out: bfloat16 [16384, 2048], P(('sp', 'tp'))
All inputs are finite; a program needn't handle non-finite values.
Results may differ from a plain program's by a relative error of at most 0.0095.
Values may be sent and summed in bfloat16 or wider, within the bound.
No kernel may reach another device: no remote copies, remote signals or barrier semaphores. Data moves between devices by JAX's collectives and lax.ppermute only.
A program may use at most 128 MiB of HBM per device.

v0:
```python
import jax
import jax.numpy as jnp
from jax import lax
from jax.sharding import PartitionSpec as P

NOPE = 128
ROPE = 64
VDIM = 128


norm_eps = 1e-06
masked_score = -1e30
theta_base = 10000.0


def in_one_piece(arrays, axis, dim, along):
    both = jnp.concatenate(arrays, axis=along)
    filled, at, gathered = (lax.all_gather(both, axis, axis=dim, tiled=True), 0, [])
    for a in arrays:
        gathered.append(lax.slice_in_dim(filled, at, at + a.shape[along], axis=along))
        at += a.shape[along]
    return tuple(gathered)


def split_up(array, dim, count):
    lengths = array.shape
    tiles = array.reshape(*lengths[:dim], count, lengths[dim] // count, *lengths[dim + 1 :])
    return jnp.moveaxis(tiles, dim, 0)


def summed_on_arrival(array, axis, dim):
    tiles = split_up(array, dim, lax.axis_size(axis))
    arrived = lax.all_to_all(tiles, axis, split_axis=0, concat_axis=0, tiled=True)
    return arrived.astype(jnp.float32).sum(axis=0)


def rotate(values_in, angle):
    half_width = values_in.shape[-1] // 2
    front_half = values_in[..., :half_width]
    back_half = values_in[..., half_width:]
    cosine = jnp.cos(angle)
    sine_part = jnp.sin(angle)
    return jnp.concatenate(
        [front_half * cosine - back_half * sine_part, back_half * cosine + front_half * sine_part],
        axis=-1,
    )


def angles(positions, full_width):
    half_width = full_width // 2
    frequency = theta_base ** (-2.0 * jnp.arange(half_width).astype(jnp.float32) / full_width)
    return positions[:, None] * frequency[None, :]


def rms_scale(values_in, gain):
    return (
        values_in
        * lax.rsqrt(jnp.mean(values_in * values_in, axis=-1, keepdims=True) + norm_eps)
        * gain
    )


def attend(fold_state, queries, key_block, value_block, rope_block, block_start):
    nope_query, rope_query, query_rows = queries
    running_max, weight_sum, accumulated = fold_state
    key_rows = block_start + jnp.arange(key_block.shape[0], dtype=jnp.int32)
    causal = key_rows[None, :] <= query_rows[:, None]
    scores = jnp.einsum("qhd,khd->hqk", nope_query, key_block, preferred_element_type=jnp.float32)
    scores = scores + jnp.einsum(
        "qhr,kr->hqk", rope_query, rope_block, preferred_element_type=jnp.float32
    )
    scores = jnp.where(causal[None], scores * (NOPE + ROPE) ** (-0.5), masked_score)
    new_max = jnp.maximum(running_max, jnp.max(scores, axis=-1))
    weights = jnp.where(causal[None], jnp.exp(scores - new_max[..., None]), 0.0)
    factor = jnp.exp(running_max - new_max)
    weight_sum = weight_sum * factor + jnp.sum(weights, axis=-1)
    accumulated = accumulated * factor[..., None] + jnp.einsum(
        "hqk,khd->hqd",
        weights.astype(jnp.bfloat16),
        value_block,
        preferred_element_type=jnp.float32,
    )
    return (new_max, weight_sum, accumulated)


def over_blocks(fold_state, arrays, last_query, step_fn, row_count):
    piece_rows = arrays[0].shape[0]
    candidates = [
        row_count * multiple
        for multiple in (4, 2, 1)
        if piece_rows % (row_count * multiple) == 0 and row_count * multiple <= 2048
    ]
    block_rows = candidates[0]
    block_count = piece_rows // block_rows
    stacked = tuple(
        (member.reshape((block_count, block_rows) + member.shape[1:]) for member in arrays)
    )

    def advance(state_in, indexed):
        block_index, blocks_now = indexed
        block_start = block_index * block_rows

        def compute(state_now):
            return step_fn(state_now, blocks_now, block_start)

        def unchanged(state_now):
            return state_now

        return (lax.cond(block_start <= last_query, compute, unchanged, state_in), None)

    result, ignored = lax.scan(
        advance, fold_state, (jnp.arange(block_count, dtype=jnp.int32), stacked)
    )
    return result


def on_device(
    resid,
    query_nope,
    query_rope,
    latent,
    key_rope,
    latent_gain,
    w_key,
    w_value,
    w_out,
    mix_gain,
    w_gate,
    w_up,
    w_down,
):
    row_count = query_nope.shape[0]
    head_count = query_nope.shape[1] // NOPE
    first_row = lax.axis_index("sp") * row_count
    query_rows = first_row + jnp.arange(row_count, dtype=jnp.int32)
    angle = angles(query_rows.astype(jnp.float32), ROPE)
    nope_query = query_nope.reshape(row_count, head_count, NOPE)
    rope_query = rotate(
        query_rope.astype(jnp.float32).reshape(row_count, head_count, ROPE), angle[:, None, :]
    ).astype(jnp.bfloat16)
    latent_normed = rms_scale(latent.astype(jnp.float32), latent_gain).astype(jnp.bfloat16)
    key_rotated = rotate(key_rope.astype(jnp.float32), angle).astype(jnp.bfloat16)
    queries = (nope_query, rope_query, query_rows)
    last_query = first_row + row_count - 1
    initial = (
        jnp.full((head_count, row_count), masked_score, jnp.float32),
        jnp.zeros((head_count, row_count), jnp.float32),
        jnp.zeros((head_count, row_count, VDIM), jnp.float32),
    )
    gate_full, up_full, down_full = in_one_piece((w_gate, w_up, w_down), "sp", 0, 1)

    def expand_block(state_now, blocks_now, block_start):
        latent_block, rope_block = blocks_now
        key_block = jnp.dot(latent_block, w_key, preferred_element_type=jnp.float32).astype(
            jnp.bfloat16
        )
        value_block = jnp.dot(latent_block, w_value, preferred_element_type=jnp.float32).astype(
            jnp.bfloat16
        )
        return attend(
            state_now,
            queries,
            key_block.reshape(-1, head_count, NOPE),
            value_block.reshape(-1, head_count, VDIM),
            rope_block,
            block_start,
        )

    final_state = over_blocks(
        initial,
        in_one_piece((latent_normed, key_rotated), "sp", 0, 1),
        last_query,
        expand_block,
        row_count,
    )
    head_out = (final_state[2] / final_state[1][..., None]).astype(jnp.bfloat16)
    out_heads = w_out.reshape(head_count, VDIM, w_out.shape[1])
    part_rows = head_out
    head_term = jnp.einsum("hqv,hvd->qd", part_rows, out_heads, preferred_element_type=jnp.float32)
    attention_proj = summed_on_arrival(
        lax.optimization_barrier(head_term.astype(jnp.bfloat16))
        .astype(jnp.float32)
        .astype(jnp.bfloat16),
        "tp",
        0,
    )
    stream = resid.astype(jnp.float32) + attention_proj
    normed = rms_scale(stream, mix_gain).astype(jnp.bfloat16)
    row_piece = lax.all_gather(normed, "tp", axis=0, tiled=True)
    gate_value = jnp.dot(row_piece, gate_full, preferred_element_type=jnp.float32)
    upward = jnp.dot(row_piece, up_full, preferred_element_type=jnp.float32)
    hidden = (jax.nn.silu(gate_value) * upward).astype(jnp.bfloat16)
    part_rows = hidden
    down_term = lax.dot_general(
        part_rows, down_full, (((1,), (1,)), ((), ())), preferred_element_type=jnp.float32
    )
    mixer_out = lax.psum_scatter(
        lax.optimization_barrier(down_term.astype(jnp.bfloat16))
        .astype(jnp.float32)
        .astype(jnp.bfloat16),
        "tp",
        scatter_dimension=0,
        tiled=True,
    ).astype(jnp.float32)
    return (stream + 0.5 * mixer_out).astype(jnp.bfloat16)


def solution(mesh):
    return jax.shard_map(
        on_device,
        mesh=mesh,
        in_specs=(
            P(("sp", "tp"), None),
            P("sp", "tp"),
            P("sp", "tp"),
            P("sp", None),
            P("sp", None),
            P(),
            P(None, "tp"),
            P(None, "tp"),
            P("tp", None),
            P(),
            P("sp", "tp"),
            P("sp", "tp"),
            P("sp", "tp"),
        ),
        out_specs=P(("sp", "tp"), None),
        check_vma=False,
    )
```

profile of v0, /device:TPU:0, one launch (start us, length us, event | category | flops | bytes accessed | tf_op | source)
XLA Modules:
  0.0 639.9 jit_solution(16293472215441492424)
XLA Ops:
  6.6 1.1 convert_element_type.78
  7.7 0.6 multiply_cosine_fusion
  8.3 0.2 copy.23
  8.5 0.2 copy.24
  8.6 1.3 fusion.31
  9.9 1.2 fusion.33
  11.2 1.1 pad_maximum_fusion
  12.4 0.8 pad_maximum_fusion.1
  13.3 0.1 copy.27
  13.5 0.2 copy.25
  13.7 0.3 copy.28
  14.0 0.7 pad_maximum_fusion.2
  14.7 90.1 %all-gather.4.cloned.1.call-done = bf16[16384,320]{1,0:T(8,128)(2,1)} async-done(((bf16[1024,320]{1,0:T(8,128)(2,1)}), bf16[16384,320]{1,0:T(8,128)(2,1)}) %all-gather.4.cloned.1.call-update) | async-done | bytes 10485776 | tf_op jit(solution)/shard_map/all_gather | solution.py:18
  104.9 3.7 slice.39
  108.5 4.8 copy.29
  113.3 7.1 %slice.38 = bf16[16384,256]{1,0:T(8,128)(2,1)} slice(bf16[16384,320]{1,0:T(8,128)(2,1)} %all-gather.4.cloned.1.call-done), slice={[0:16384], [0:256]} | slice | bytes 16777216 | tf_op jit(solution)/shard_map/slice | solution.py:20
  120.4 0.6 iota.20
  121.0 1.1 broadcast_in_dim.50
  122.1 0.6 broadcast_in_dim.49
  122.7 59.4 %while.15 = (s32[]{:T(128)}, f32[2,1024]{1,0:T(2,128)S(1)}, f32[2,1024]{1,0:T(2,128)}, f32[2,1024,128]{2,1,0:T(8,128)}, s32[8]{0:T(128)}, /*index=5*/s32[]{:T(12...) while((s32[]{:T(128)}, f32[2,1024]{1,0:T(2,128)S(1)}, ...), condition=%wide.region_6.7_spmd.clone, body=%wide.region_1.6_spmd.clone.sunk | while | flops 3266845696 | bytes 178161584 | solution.py:111
  122.7 1.3 dynamic_slice.38
  124.6 43.7 %conditional.3 = ((f32[2,1024]{1,0:T(2,128)S(1)}, f32[2,1024]{1,0:T(2,128)}, f32[2,1024,128]{2,1,0:T(8,128)})) conditional(s32[]{:T(128)} %convert_element_type.126, (f32[2,1024]{1,0:T(2,128)S(1)}, f32[2,1024]{1,0:T(2,128)}, f32[2,1024,128]{2,1,0:T(8,128)}) %tuple.44, (s32[]{:T(128)}, s32[]{:T(128)}, bf16[8,2048,256]{2,1,0:T(8,128)(2,1)}, s32[]{:T(128)}, ...), branch_computations={%region_2.2_spmd, %region_3.5_spmd} | conditional | flops 3266845696 | bytes 178157184 | solution.py:109
  124.6 1.8 convolution_convert_fusion.1
  126.4 8.1 %fusion.37 = f32[2,2048,1024]{2,1,0:T(8,128)} fusion(bf16[2048,2,128]{0,2,1:T(8,128)(2,1)S(1)} %bitcast.42, bf16[1024,2,128]{2,0,1:T(8,128)(2,1)S(1)} %get-tuple-element.152), kind=kOutput, calls=%fused_computation.62 | convolution fusion | flops 1073741824 | bytes 18350080 | tf_op jit(solution)/shard_map/while/body/eval_jaxpr/cond/branch_1_fun/qhd,khd->hqk/dot_general | solution.py:68
  134.5 1.3 broadcast_compare_fusion
  135.9 12.3 %fusion.36 = (f32[2,1024]{1,0:T(2,128)S(1)}, f32[2,1024,2048]{1,2,0:T(8,128)}) fusion(bf16[1024,2,64]{0,2,1:T(8,128)(2,1)} %get-tuple-element.154, bf16[8,2048,64]{1,2,0:T(8,128)(2,1)} %get-tuple-element.153, s32[]{:T(128)} %get-tuple-element.150, f32[2,2048,1024]{2,1,0:T(8,128)} %fusion.37, pred[1024,2048]{0,1:T(8,128)(4,1)S(1)} %broadcast_compare_fusion), kind=kOutput, calls=%fused_computation.61 | convolution fusion | flops 553646080 | bytes 36184576 | tf_op jit(solution)/shard_map/while/body/eval_jaxpr/cond/branch_1_fun/qhr,kr->hqk/dot_general | solution.py:69
  148.2 8.6 %fusion.5 = f32[2,1024]{1,0:T(2,128)S(1)} fusion(f32[2,1024,2048]{1,2,0:T(8,128)} %get-tuple-element.256, f32[2,1024]{1,0:T(2,128)S(1)} %max.4, pred[1024,2048]{0,1:T(8,128)(4,1)} %copy-done.2), kind=kLoop, calls=%fused_computation.6 | loop fusion | flops 12580864 | bytes 18890752 | tf_op jit(solution)/shard_map/while/body/eval_jaxpr/cond/branch_1_fun/reduce_sum | solution.py:76
  156.8 2.1 multiply_add_fusion
  158.9 1.8 convolution_convert_fusion
  160.6 7.7 %fusion.9 = f32[2,1024,128]{2,1,0:T(8,128)} fusion(bf16[2048,2,128]{0,2,1:T(8,128)(2,1)S(1)} %bitcast.44, f32[2,1024,2048]{1,2,0:T(8,128)S(1)} %copy-done.1, f32[2,1024]{1,0:T(2,128)S(1)} %max.4, pred[1024,2048]{0,1:T(8,128)(4,1)} %copy-done.2, f32[2,1024,128]{2,1,0:T(8,128)} %get-tuple-element.156, f32[2,1024]{1,0:T(2,128)S(1)} %get-tuple-element.254), kind=kOutput, calls=%fused_computation.12 | convolution fusion | flops 1086849024 | bytes 22036480 | tf_op jit(solution)/shard_map/while/body/eval_jaxpr/cond/branch_1_fun/hqk,khd->hqd/dot_general | solution.py:77
  168.3 1.3 dynamic_slice.38
  170.3 1.3 dynamic_slice.38
  172.2 1.3 dynamic_slice.38
  174.2 1.3 dynamic_slice.38
  176.2 1.3 dynamic_slice.38
  178.1 1.3 dynamic_slice.38
  180.1 1.3 dynamic_slice.38
  182.1 2.5 bitcast_convert_fusion
  184.6 53.7 %all_to_all.5 = bf16[8,128,2048]{2,1,0:T(8,128)(2,1)S(1)} all-to-all(bf16[8,128,2048]{2,1,0:T(8,128)(2,1)S(1)} %bitcast.46), channel_id=1, replica_groups=mesh['sp'=16,'tp'=8] {'tp'}, dimensions={0} | all-to-all | bytes 8388608 | tf_op jit(solution)/shard_map/all_to_all | solution.py:33
  238.4 0.7 convert_reduce_fusion
  239.1 0.3 copy-done.3
  239.4 0.2 multiply_reduce_fusion
  239.6 1.0 multiply_convert_fusion.1
  240.7 332.6 %all-gather.6.cloned.1.call-done = bf16[1024,2048]{1,0:T(8,128)(2,1)} async-done(((bf16[128,2048]{1,0:T(8,128)(2,1)}), bf16[1024,2048]{1,0:T(8,128)(2,1)}) %all-gather.6.cloned.1.call-update) | async-done | bytes 4194320 | tf_op jit(solution)/shard_map/all_gather | solution.py:189
  573.4 7.9 %fusion.25 = f32[1024,704]{0,1:T(8,128)} fusion(bf16[1024,2048]{1,0:T(8,128)(2,1)} %all-gather.6.cloned.1.call-done, bf16[2048,2112]{0,1:T(8,128)(2,1)} %all-gather.8.cloned.1.call-done), kind=kOutput, calls=%fused_computation.33 | convolution fusion | flops 2952790016 | bytes 9961472 | tf_op jit(solution)/shard_map/dot_general | solution.py:190
  581.3 12.0 %convolution_convert_fusion.2 = bf16[1024,2048]{1,0:T(8,128)(2,1)} fusion(bf16[2048,2112]{0,1:T(8,128)(2,1)} %all-gather.8.cloned.1.call-done, f32[1024,704]{0,1:T(8,128)} %fusion.25, bf16[1024,2048]{1,0:T(8,128)(2,1)} %all-gather.6.cloned.1.call-done), kind=kOutput, calls=%fused_computation.29 | convolution fusion | flops 5912002560 | bytes 17039360 | tf_op jit(solution)/shard_map/dot_general | solution.py:194
  593.3 38.0 %reduce-scatter.2.cloned.1.call-done = bf16[128,2048]{1,0:T(8,128)(2,1)} async-done(((bf16[1024,2048]{1,0:T(8,128)(2,1)}), bf16[128,2048]{1,0:T(8,128)(2,1)}) %reduce-scatter.2.cloned.1.call-update) | async-done | bytes 524304 | tf_op jit(solution)/shard_map/reduce_scatter | solution.py:197
  631.3 2.0 add_convert_fusion
  (55 shorter events, 0.5 us)
Async XLA Ops:
  6.5 175.5 %copy-start = (bf16[256,2048]{1,0:T(8,128)(2,1)S(1)}, bf16[256,2048]{1,0:T(8,128)(2,1)}, u32[]{:S(2)}) copy-start(bf16[256,2048]{1,0:T(8,128)(2,1)} %param.25) | copy-start | bytes 3145732
  6.5 5.8 copy-start.9
  6.5 5.8 copy-start.8
  6.5 5.8 copy-start.7
  6.5 6.7 %copy-start.6 = (bf16[1024,128]{1,0:T(8,128)(2,1)S(1)}, bf16[1024,128]{1,0:T(8,128)(2,1)}, u32[]{:S(2)}) copy-start(bf16[1024,128]{1,0:T(8,128)(2,1)} %param.19) | copy-start | bytes 786436
  6.5 6.9 %copy-start.5 = (bf16[1024,256]{1,0:T(8,128)(2,1)S(1)}, bf16[1024,256]{1,0:T(8,128)(2,1)}, u32[]{:S(2)}) copy-start(bf16[1024,256]{1,0:T(8,128)(2,1)} %param.18) | copy-start | bytes 1572868
  6.6 98.3 %all-gather.4.cloned.1.call-start = ((), (), s32[]{:S(2)}) async-start(), calls=%async_computation.2 | async-start | bytes 13369344 | tf_op jit(solution)/shard_map/all_gather | solution.py:18
  12.3 228.4 %all-gather.8.cloned.1.call-start = ((), (), s32[]{:S(2)}) async-start(), calls=%async_computation.4 | async-start | bytes 9191424 | tf_op jit(solution)/shard_map/all_gather | solution.py:18
  13.2 560.1 %all-gather.6.cloned.1.call-start = ((), (), s32[]{:S(2)}) async-start(), calls=%async_computation.3 | async-start | bytes 4718592 | tf_op jit(solution)/shard_map/all_gather | solution.py:189
  135.9 12.3 %copy-start.2 = (pred[1024,2048]{0,1:T(8,128)(4,1)}, pred[1024,2048]{0,1:T(8,128)(4,1)S(1)}, u32[]{:S(2)}) copy-start(pred[1024,2048]{0,1:T(8,128)(4,1)S(1)} %broadcast_compare_fusion) | copy-start | bytes 6291460 | tf_op jit(solution)/shard_map/while/body/eval_jaxpr/cond
  148.2 10.7 %copy-start.4 = (bf16[256,256]{1,0:T(8,128)(2,1)S(1)}, bf16[256,256]{1,0:T(8,128)(2,1)}, u32[]{:S(2)}) copy-start(bf16[256,256]{1,0:T(8,128)(2,1)} %get-tuple-element.157) | copy-start | bytes 393220 | tf_op jit(solution)/shard_map/while/body/eval_jaxpr/cond
  148.2 12.5 %copy-start.1 = (f32[2,1024,2048]{1,2,0:T(8,128)S(1)}, f32[2,1024,2048]{1,2,0:T(8,128)}, u32[]{:S(2)}) copy-start(f32[2,1024,2048]{1,2,0:T(8,128)} %get-tuple-element.256) | copy-start | bytes 50331652 | tf_op jit(solution)/shard_map/while/body/eval_jaxpr/cond
  238.4 1.0 copy-start.3
  238.4 1.3 copy-start.10
  240.6 390.7 %reduce-scatter.2.cloned.1.call-start = ((), (), s32[]{:S(2)}) async-start(), calls=%async_computation.5 | async-start | bytes 4718592 | tf_op jit(solution)/shard_map/reduce_scatter | solution.py:197
Sparse Core Ops, SparseCore 0:
  12.4 92.3 all-gather.3
  107.0 78.2 all-gather.7
  240.7 332.5 all-gather.5
  593.4 37.8 reduce-scatter.1
where the time goes:
time: 641 us; the launch traced here: 640 us
  waiting for transfers between devices  461 us (72%)
  matrix products  54 us (8%)
  blocking collectives  53.7 us (8%)
  local copies, waits for them, and re-layouts  29.4 us (5%)
  other arithmetic  22.9 us (4%)
  between operations  13.3 us (2%)
    all_gather x1, waiting for transfers between devices, on_device(): row_piece = lax.all_gather(normed, 'tp', axis=0, tiled=True)  333 us
    all_gather x2, waiting for transfers between devices, in_one_piece(): lax.all_gather(both, axis, axis=dim, tiled=True)  90.1 us
    all_to_all x1, blocking collectives, summed_on_arrival(): lax.all_to_all(tiles, axis, split_axis=0, concat_axis=0, tiled=True)  53.7 us
    reduce_scatter x1, waiting for transfers between devices, on_device(): lax.psum_scatter(lax.optimization_barrier(down_term.astype(jnp.bfloat16))...  38 us
  transfers between devices with their start and end apart: 4, of which 3 were waited for; matrix products, arithmetic and copies ran while one was open for 12% of the time, Pallas kernels for 0%

commit v1 on v0

v1 whole, which is shorter than its diff:
```python
import functools

import jax
import jax.numpy as jnp
from jax import lax
from jax.experimental import pallas as pl
from jax.experimental.pallas import tpu as pltpu
from jax.sharding import PartitionSpec as P

NOPE = 128
ROPE = 64
VDIM = 128
TILE = 256
LOG2E = 1.4426950408889634

norm_eps = 1e-06
masked_score = -1e30
theta_base = 10000.0


def rotate(values_in, angle):
    half_width = values_in.shape[-1] // 2
    front_half = values_in[..., :half_width]
    back_half = values_in[..., half_width:]
    cosine = jnp.cos(angle)
    sine_part = jnp.sin(angle)
    return jnp.concatenate(
        [front_half * cosine - back_half * sine_part, back_half * cosine + front_half * sine_part],
        axis=-1,
    )


def angles(positions, full_width):
    half_width = full_width // 2
    frequency = theta_base ** (-2.0 * jnp.arange(half_width).astype(jnp.float32) / full_width)
    return positions[:, None] * frequency[None, :]


def rms_scale(values_in, gain):
    return (
        values_in
        * lax.rsqrt(jnp.mean(values_in * values_in, axis=-1, keepdims=True) + norm_eps)
        * gain
    )


def attention_kernel(rows, lo_ref, block_ref, qa_ref, qb_ref, wkv_ref, out_ref, k_ref, v_ref, m_ref, acc_ref):
    step = pl.program_id(0)
    steps = pl.num_programs(0)
    low = lo_ref[0]
    high = steps - 1 - low
    tiles = rows // TILE
    scale = (NOPE + ROPE) ** (-0.5) * LOG2E

    @pl.when(step == 0)
    def _():
        m_ref[...] = jnp.full(m_ref.shape, masked_score, jnp.float32)
        acc_ref[...] = jnp.zeros(acc_ref.shape, jnp.float32)
        v_ref[:, VDIM:] = jnp.ones((rows, VDIM), jnp.bfloat16)

    def scores(row_start, part):
        q_ref = qa_ref if part % 2 == 0 else qb_ref
        return lax.dot_general(
            q_ref[pl.ds(row_start, TILE), :],
            k_ref[part * TILE : (part + 1) * TILE, :],
            (((1,), (1,)), ((), ())),
            preferred_element_type=jnp.float32,
        )

    def fold(row_start, parts, diagonal):
        s = [scores(row_start, part) * scale for part in range(parts)]
        if diagonal:
            row = lax.broadcasted_iota(jnp.int32, (TILE, TILE), 0)
            col = lax.broadcasted_iota(jnp.int32, (TILE, TILE), 1)
            s[-1] = jnp.where(col <= row, s[-1], masked_score)
        top = s[0]
        for other in s[1:]:
            top = jnp.maximum(top, other)
        old_max = m_ref[pl.ds(row_start, TILE), :]
        new_max = jnp.maximum(old_max, jnp.max(top, axis=-1, keepdims=True))
        factor = jnp.exp2(old_max - new_max)
        wide_max = jnp.concatenate([new_max, new_max], axis=1)
        total = jnp.concatenate([factor, factor], axis=1) * acc_ref[pl.ds(row_start, TILE), :]
        for part in range(parts):
            weights = jnp.exp2(s[part] - wide_max).astype(jnp.bfloat16)
            total = total + jnp.dot(
                weights,
                v_ref[part * TILE : (part + 1) * TILE, :],
                preferred_element_type=jnp.float32,
            )
        m_ref[pl.ds(row_start, TILE), :] = new_max
        acc_ref[pl.ds(row_start, TILE), :] = total

    @pl.when(step <= high)
    def _():
        expanded = jnp.dot(
            block_ref[0, :rows, :], wkv_ref[...], preferred_element_type=jnp.float32
        ).astype(jnp.bfloat16)
        k_ref[:, :NOPE] = expanded[:, :NOPE]
        v_ref[:, :VDIM] = expanded[:, NOPE:]
        for part in range(tiles):
            k_ref[part * TILE : (part + 1) * TILE, NOPE:] = block_ref[
                0, rows:, (part // 2) * 128 : (part // 2 + 1) * 128
            ]

        first = jnp.where(step < low, 0, 1)
        last = jnp.where(step < high, 2, 1)

        def whole(group, carry):
            base = group * rows
            for tile in range(tiles):
                fold(pl.multiple_of(base + tile * TILE, TILE), tiles, False)
            return carry

        lax.fori_loop(first, last, whole, 0)

        @pl.when((step == low) | (step == high))
        def _():
            base = jnp.where(step == low, 0, rows)
            for tile in range(tiles):
                fold(pl.multiple_of(base + tile * TILE, TILE), tile + 1, True)

    @pl.when(step == steps - 1)
    def _():
        out_ref[...] = (acc_ref[:, :VDIM] / acc_ref[:, VDIM:]).astype(jnp.bfloat16)


def attention(low, blocks, query_a, query_b, w_kv):
    count, packed_rows, width = blocks.shape
    rows = query_a.shape[0] // 2
    return pl.pallas_call(
        functools.partial(attention_kernel, rows),
        grid_spec=pltpu.PrefetchScalarGridSpec(
            num_scalar_prefetch=1,
            grid=(count,),
            in_specs=[
                pl.BlockSpec((1, packed_rows, width), lambda i, lo: (jnp.minimum(i, count - 1 - lo[0]), 0, 0)),
                pl.BlockSpec(query_a.shape, lambda i, lo: (0, 0)),
                pl.BlockSpec(query_b.shape, lambda i, lo: (0, 0)),
                pl.BlockSpec(w_kv.shape, lambda i, lo: (0, 0)),
            ],
            out_specs=pl.BlockSpec((2 * rows, VDIM), lambda i, lo: (0, 0)),
            scratch_shapes=[
                pltpu.VMEM((rows, NOPE + 128), jnp.bfloat16),
                pltpu.VMEM((rows, 2 * VDIM), jnp.bfloat16),
                pltpu.VMEM((2 * rows, 128), jnp.float32),
                pltpu.VMEM((2 * rows, 2 * VDIM), jnp.float32),
            ],
        ),
        out_shape=jax.ShapeDtypeStruct((2 * rows, VDIM), jnp.bfloat16),
        compiler_params=pltpu.CompilerParams(dimension_semantics=("arbitrary",)),
        cost_estimate=pl.CostEstimate(
            flops=17 * rows * rows * 1024, bytes_accessed=blocks.size * 2, transcendentals=17 * rows * rows
        ),
        name="attention",
    )(low, blocks, query_a, query_b, w_kv)


def on_device(
    resid,
    query_nope,
    query_rope,
    latent,
    key_rope,
    latent_gain,
    w_key,
    w_value,
    w_out,
    mix_gain,
    w_gate,
    w_up,
    w_down,
):
    n_sp = lax.axis_size("sp")
    n_tp = lax.axis_size("tp")
    rows = query_nope.shape[0]
    here = lax.axis_index("sp")
    upper = here >= n_sp // 2
    first_row = here * rows
    angle = angles((first_row + jnp.arange(rows, dtype=jnp.int32)).astype(jnp.float32), ROPE)

    latent_normed = rms_scale(latent.astype(jnp.float32), latent_gain).astype(jnp.bfloat16)
    key_rotated = rotate(key_rope.astype(jnp.float32), angle).astype(jnp.bfloat16)
    packed_rope = jnp.concatenate(jnp.split(key_rotated, 4, axis=0), axis=1)
    own_block = jnp.concatenate([latent_normed, packed_rope], axis=0)
    blocks = lax.all_gather(own_block, "sp", axis=0, tiled=False)
    weights_full = lax.all_gather(
        jnp.concatenate([w_gate, w_up, w_down], axis=1), "sp", axis=0, tiled=True
    )
    out_full = lax.all_gather(w_out, "tp", axis=0, tiled=True)

    rope_query = rotate(
        query_rope.astype(jnp.float32).reshape(rows, 2, ROPE), angle[:, None, :]
    ).astype(jnp.bfloat16)
    blank = jnp.zeros((rows, ROPE), jnp.bfloat16)
    by_head = [
        jnp.concatenate([query_nope[:, h * NOPE : (h + 1) * NOPE], rope_query[:, h], blank], axis=1)
        for h in range(2)
    ]
    kept = jnp.where(upper, by_head[1], by_head[0])
    given = jnp.where(upper, by_head[0], by_head[1])
    partner = [(i, n_sp - 1 - i) for i in range(n_sp)]
    taken = lax.ppermute(given, "sp", partner)
    query_a = jnp.where(
        upper, jnp.concatenate([taken, kept], axis=0), jnp.concatenate([kept, taken], axis=0)
    )
    query_b = jnp.concatenate([query_a[:, :NOPE], query_a[:, NOPE + ROPE :], query_a[:, NOPE : NOPE + ROPE]], axis=1)
    w_kv = jnp.where(
        upper,
        jnp.concatenate([w_key[:, NOPE:], w_value[:, VDIM:]], axis=1),
        jnp.concatenate([w_key[:, :NOPE], w_value[:, :VDIM]], axis=1),
    )
    low = jnp.minimum(here, n_sp - 1 - here).astype(jnp.int32).reshape(1)
    head_out = attention(low, blocks, query_a, query_b, w_kv)

    groups = [
        [b * n_tp + t for b in (p, n_sp - 1 - p) for t in range(n_tp)] for p in range(n_sp // 2)
    ]
    piece = rows // n_tp
    arrived = lax.all_to_all(
        head_out.reshape(2 * n_tp, piece, VDIM),
        ("sp", "tp"),
        split_axis=0,
        concat_axis=0,
        axis_index_groups=groups,
        tiled=True,
    )
    all_heads = arrived.reshape(2, n_tp, piece, VDIM).transpose(2, 1, 0, 3).reshape(piece, 2 * n_tp * VDIM)
    attention_proj = jnp.dot(all_heads, out_full, preferred_element_type=jnp.float32)
    stream = resid.astype(jnp.float32) + attention_proj
    normed = rms_scale(stream, mix_gain).astype(jnp.bfloat16)
    row_piece = lax.all_gather(normed, "tp", axis=0, tiled=True)
    units = w_gate.shape[1]
    gate_value = jnp.dot(row_piece, weights_full[:, :units], preferred_element_type=jnp.float32)
    upward = jnp.dot(row_piece, weights_full[:, units : 2 * units], preferred_element_type=jnp.float32)
    hidden = (jax.nn.silu(gate_value) * upward).astype(jnp.bfloat16)
    down_term = lax.dot_general(
        hidden, weights_full[:, 2 * units :], (((1,), (1,)), ((), ())), preferred_element_type=jnp.float32
    )
    mixer_out = lax.psum_scatter(
        down_term.astype(jnp.bfloat16), "tp", scatter_dimension=0, tiled=True
    ).astype(jnp.float32)
    return (stream + 0.5 * mixer_out).astype(jnp.bfloat16)


def solution(mesh):
    return jax.shard_map(
        on_device,
        mesh=mesh,
        in_specs=(
            P(("sp", "tp"), None),
            P("sp", "tp"),
            P("sp", "tp"),
            P("sp", None),
            P("sp", None),
            P(),
            P(None, "tp"),
            P(None, "tp"),
            P("tp", None),
            P(),
            P("sp", "tp"),
            P("sp", "tp"),
            P("sp", "tp"),
        ),
        out_specs=P(("sp", "tp"), None),
        check_vma=False,
    )
```

time: 641 us -> 337 us (0.53)
  waiting for transfers between devices: 461 us -> 217 us
  Pallas kernels: 0 us -> 38.7 us
  blocking collectives: 53.7 us -> 20.9 us
  matrix products: 54 us -> 24.7 us
  local copies, waits for them, and re-layouts: 29.4 us -> 2.57 us
  other arithmetic: 22.9 us -> 11.9 us
  starting transfers between devices: 0.16 us -> 7.02 us
    all_gather x1, waiting for transfers between devices: 333 us -> 32.8 us  [on_device(): row_piece = lax.all_gather(normed, 'tp', axis=0, tiled=True)]
    pallas_call x0 -> x1, Pallas kernels: none -> 38.7 us  [attention(): pl.pallas_call(functools.partial(attention_kernel, rows), grid_spec=pltpu...]
    all_gather x2 -> x3, waiting for transfers between devices: 90.1 us -> 125 us  [the longest x1 70.5 us: on_device(): lax.all_gather(jnp.concatenate([w_gate, w_up, w_down], axis=1), 'sp', axi...]
    all_to_all x1, blocking collectives: 53.7 us -> 20.9 us  [on_device(): lax.all_to_all(head_out.reshape(2 * n_tp, piece, VDIM), ('sp', 'tp'), spl...]
    dot_general x8 -> x3, matrix products: 54 us -> 24.7 us  [the longest x1 12 us: on_device(): lax.dot_general(hidden, weights_full[:, 2 * units:], (((1,), (1,)), ((),...]
    ppermute x0 -> x1, waiting for transfers between devices: none -> 20.4 us  [on_device(): taken = lax.ppermute(given, 'sp', partner)]
    slice x2 -> x5, local copies, waits for them, and re-layouts: 10.8 us -> 0.41 us  [the longest x1 0.25 us: on_device(): query_a[:, NOPE + ROPE:]]
    dynamic_slice x8 -> x0, local copies, waits for them, and re-layouts: 10.2 us -> none  [over_blocks(): lax.scan(advance, fold_state, (jnp.arange(block_count, dtype=jnp.int32),...]
  transfers between devices with their start and end apart: 4 -> 6, of which waited for: 3 -> 5; matrix products, arithmetic and copies ran while one was open for 12% -> 3% of each run, Pallas kernels for 0% -> 12%
where the time goes in v1:
time: 337 us
  waiting for transfers between devices  217 us (64%)
  Pallas kernels  38.7 us (11%)
  matrix products  24.7 us (7%)
  blocking collectives  20.9 us (6%)
  between operations  13.4 us (4%)
  other arithmetic  11.9 us (4%)
  starting transfers between devices  7.02 us (2%)
    all_gather x1, waiting for transfers between devices, on_device(): lax.all_gather(jnp.concatenate([w_gate, w_up, w_down], axis=1), 'sp', axi...  70.5 us
    all_gather x1, waiting for transfers between devices, on_device(): blocks = lax.all_gather(own_block, 'sp', axis=0, tiled=False)  54.6 us
    pallas_call x1, Pallas kernels, attention(): pl.pallas_call(functools.partial(attention_kernel, rows), grid_spec=pltpu...  38.7 us
    reduce_scatter x1, waiting for transfers between devices, on_device(): lax.psum_scatter(down_term.astype(jnp.bfloat16), 'tp', scatter_dimension=...  38 us
    all_gather x1, waiting for transfers between devices, on_device(): row_piece = lax.all_gather(normed, 'tp', axis=0, tiled=True)  32.8 us
    all_to_all x1, blocking collectives, on_device(): lax.all_to_all(head_out.reshape(2 * n_tp, piece, VDIM), ('sp', 'tp'), spl...  20.9 us
    ppermute x1, waiting for transfers between devices, on_device(): taken = lax.ppermute(given, 'sp', partner)  20.4 us
    dot_general x1, matrix products, on_device(): lax.dot_general(hidden, weights_full[:, 2 * units:], (((1,), (1,)), ((),...  12 us
  transfers between devices with their start and end apart: 6, of which 5 were waited for; matrix products, arithmetic and copies ran while one was open for 3% of the time, Pallas kernels for 12%

profile of v1, /device:TPU:0, one launch (start us, length us, event | category | flops | bytes accessed | tf_op | source)
XLA Modules:
  0.0 336.6 jit_solution(17769819414752773627)
XLA Ops:
  6.5 0.9 convert_element_type.47
  7.5 0.6 multiply_cosine_fusion
  8.1 0.0 copy-start.5
  8.1 0.0 copy-start.6
  8.1 0.1 copy.23
  8.2 1.3 fusion.9
  9.6 1.2 fusion.11
  10.8 0.9 pad_maximum_fusion.1
  11.7 0.0 all-gather.12.cloned.1.call-update
  11.8 0.0 all-gather.6.cloned.1.call-start
  11.8 0.7 all-gather.6.cloned.1.call-update
  12.5 0.0 all-gather.10.cloned.1.call-start
  12.6 0.9 pad_maximum_fusion.2
  13.4 0.0 all-gather.10.cloned.1.call-update
  13.5 0.0 all-gather.8.cloned.1.call-start
  13.5 0.2 copy.26
  13.7 0.2 copy.28
  13.9 0.1 copy.24
  14.1 0.3 copy.30
  14.5 0.3 copy.31
  14.8 0.1 pad.19.clone
  14.9 0.3 subtract_convert_fusion
  15.2 0.0 copy-start.7
  15.2 0.3 fusion.13
  15.5 0.4 copy-done.2
  16.0 0.3 broadcast_select_fusion.1
  16.3 6.7 %collective-permute-start = (bf16[1024,256]{1,0:T(8,128)(2,1)S(1)}, bf16[1024,256]{1,0:T(8,128)(2,1)S(1)}, u32[]{:S(2)}, u32[]{:S(2)}) collective-permute-start(bf16[1024,256]{1,0:T(8,128)(2,1)S(1)} %get-tuple-element.7), channel_id=1, source_target_pairs={{0,120},{8,112},{16,104},{24,96},{32,88},{40,80},{48,72},{56,64},{... | collective-permute-start | bytes 1572872 | tf_op jit(solution)/shard_map/ppermute | solution.py:203
  23.0 0.7 maximum_select_fusion.1.wkv_ref
  23.8 20.4 %collective-permute-done = bf16[1024,256]{1,0:T(8,128)(2,1)S(1)} collective-permute-done((bf16[1024,256]{1,0:T(8,128)(2,1)S(1)}, bf16[1024,256]{1,0:T(8,128)(2,1)S(1)}, u32[]{:S(2)}, u32[]{:S(2)}) %collective-permute-start) | collective-permute-done | bytes 524320 | tf_op jit(solution)/shard_map/ppermute | solution.py:203
  44.2 0.2 maximum_select_fusion.qa_ref
  44.5 0.2 fusion.20
  44.7 1.3 pad_maximum_fusion.qb_ref
  46.1 54.6 %all-gather.12.cloned.1.call-done = bf16[20480,256]{1,0:T(8,128)(2,1)} async-done(((bf16[1280,256]{1,0:T(8,128)(2,1)}), bf16[20480,256]{1,0:T(8,128)(2,1)}) %all-gather.12.cloned.1.call-update) | async-done | bytes 10485776 | tf_op jit(solution)/shard_map/all_gather | solution.py:186
  100.7 38.7 %attention.1 = bf16[2048,128]{1,0:T(8,128)(2,1)} custom-call(s32[1]{0:T(128)} %bitcast.lo_ref, bf16[16,1280,256]{2,1,0:T(8,128)(2,1)} %bitcast.21, bf16[2048,256]{1,0:T(8,128)(2,1)} %copy-done, bf16[2048,256]{1,0:T(8,128)(2,1)} %pad_maximum_fusion.qb_ref, bf16[256,256]{1,0:T(8,128)(2,1)} %maximum_select_fusion.1.wkv_ref), custom_call_target="tpu_custom_call" | custom-call | flops 18253611008 | bytes 10485760 | tf_op jit(solution)/shard_map/attention/pallas_call | solution.py:131
  139.4 20.9 %all_to_all.5 = bf16[16,128,128]{2,1,0:T(8,128)(2,1)S(1)} all-to-all(bf16[16,128,128]{2,1,0:T(8,128)(2,1)} %bitcast.20), channel_id=1, replica_groups={{0,1,2,3,4,5,6,7,120,121,122,123,124,125,126,127},{8,9,10,11,12,13,14,1..., dimensions={0} | all-to-all | bytes 1048576 | tf_op jit(solution)/shard_map/all_to_all | solution.py:220
  160.4 0.3 copy.29
  160.7 0.0 all-gather.6.cloned.1.call-done
  160.7 4.8 %multiply_reduce_fusion = (f32[128]{0:T(128)S(1)}, f32[128,2048]{1,0:T(8,128)S(1)}) fusion(bf16[128,2048]{0,1:T(8,128)(2,1)S(1)} %bitcast.17, bf16[2048,2048]{1,0:T(8,128)(2,1)} %all-gather.6.cloned.1.call-done, bf16[128,2048]{1,0:T(8,128)(2,1)S(1)} %copy-done.1), kind=kOutput, calls=%fused_computation.17 | convolution fusion | flops 1074790272 | bytes 10486272 | tf_op jit(solution)/shard_map/dot_general | solution.py:229
  165.5 1.0 multiply_convert_fusion.1
  166.5 0.0 all-gather.8.cloned.1.call-update
  166.5 0.2 reduce-scatter.2.cloned.1.call-start
  166.7 70.5 %all-gather.10.cloned.1.call-done = bf16[2048,2112]{0,1:T(8,128)(2,1)} async-done(((bf16[128,2112]{0,1:T(8,128)(2,1)}), bf16[2048,2112]{0,1:T(8,128)(2,1)}) %all-gather.10.cloned.1.call-update) | async-done | bytes 8650768 | tf_op jit(solution)/shard_map/all_gather | solution.py:187
  237.2 32.8 %all-gather.8.cloned.1.call-done = bf16[1024,2048]{1,0:T(8,128)(2,1)} async-done(((bf16[128,2048]{1,0:T(8,128)(2,1)}), bf16[1024,2048]{1,0:T(8,128)(2,1)}) %all-gather.8.cloned.1.call-update) | async-done | bytes 4194320 | tf_op jit(solution)/shard_map/all_gather | solution.py:232
  270.0 7.9 %fusion.3 = f32[1024,704]{0,1:T(8,128)} fusion(bf16[1024,2048]{1,0:T(8,128)(2,1)} %all-gather.8.cloned.1.call-done, bf16[2048,2112]{0,1:T(8,128)(2,1)} %all-gather.10.cloned.1.call-done), kind=kOutput, calls=%fused_computation.4 | convolution fusion | flops 2952790016 | bytes 9961472 | tf_op jit(solution)/shard_map/dot_general | solution.py:234
  277.9 12.0 %convolution_convert_fusion = bf16[1024,2048]{1,0:T(8,128)(2,1)} fusion(bf16[2048,2112]{0,1:T(8,128)(2,1)} %all-gather.10.cloned.1.call-done, f32[1024,704]{0,1:T(8,128)} %fusion.3, bf16[1024,2048]{1,0:T(8,128)(2,1)} %all-gather.8.cloned.1.call-done), kind=kOutput, calls=%fused_computation | convolution fusion | flops 5912002560 | bytes 17039360 | tf_op jit(solution)/shard_map/dot_general | solution.py:237
  290.0 0.0 reduce-scatter.2.cloned.1.call-update
  290.0 38.0 %reduce-scatter.2.cloned.1.call-done = bf16[128,2048]{1,0:T(8,128)(2,1)} async-done(((bf16[1024,2048]{1,0:T(8,128)(2,1)}), bf16[128,2048]{1,0:T(8,128)(2,1)}) %reduce-scatter.2.cloned.1.call-update) | async-done | bytes 524304 | tf_op jit(solution)/shard_map/reduce_scatter | solution.py:240
  328.1 2.0 add_convert_fusion
  (28 shorter events, 0.3 us)
Async XLA Ops:
  6.5 94.2 %all-gather.12.cloned.1.call-start = ((), (), s32[]{:S(2)}) async-start(), calls=%async_computation.6 | async-start | bytes 11141120 | tf_op jit(solution)/shard_map/all_gather | solution.py:186
  8.0 4.5 %copy-start.4 = (bf16[128,704]{0,1:T(8,128)(2,1)S(1)}, bf16[128,704]{0,1:T(8,128)(2,1)}, u32[]{:S(2)}) copy-start(bf16[128,704]{0,1:T(8,128)(2,1)} %param.25) | copy-start | bytes 540676
  8.1 4.5 %copy-start.5 = (bf16[128,704]{0,1:T(8,128)(2,1)S(1)}, bf16[128,704]{0,1:T(8,128)(2,1)}, u32[]{:S(2)}) copy-start(bf16[128,704]{0,1:T(8,128)(2,1)} %param.24) | copy-start | bytes 540676
  8.1 4.5 %copy-start.6 = (bf16[128,704]{0,1:T(8,128)(2,1)S(1)}, bf16[128,704]{0,1:T(8,128)(2,1)}, u32[]{:S(2)}) copy-start(bf16[128,704]{0,1:T(8,128)(2,1)} %param.23) | copy-start | bytes 540676
  10.8 3.1 copy-start.3
  11.8 148.9 %all-gather.6.cloned.1.call-start = ((), (), s32[]{:S(2)}) async-start(), calls=%async_computation.2 | async-start | bytes 9437184 | tf_op jit(solution)/shard_map/all_gather | solution.py:190
  12.5 224.7 %all-gather.10.cloned.1.call-start = ((), (), s32[]{:S(2)}) async-start(), calls=%async_computation.4 | async-start | bytes 9191424 | tf_op jit(solution)/shard_map/all_gather | solution.py:187
  13.5 256.6 %all-gather.8.cloned.1.call-start = ((), (), s32[]{:S(2)}) async-start(), calls=%async_computation.3 | async-start | bytes 4718592 | tf_op jit(solution)/shard_map/all_gather | solution.py:232
  14.9 1.0 copy-start.2
  15.2 7.8 %copy-start.7 = (bf16[256,256]{1,0:T(8,128)(2,1)S(1)}, bf16[256,256]{1,0:T(8,128)(2,1)}, u32[]{:S(2)}) copy-start(bf16[256,256]{1,0:T(8,128)(2,1)} %param.19) | copy-start | bytes 393220
  15.2 7.8 %copy-start.8 = (bf16[256,256]{1,0:T(8,128)(2,1)S(1)}, bf16[256,256]{1,0:T(8,128)(2,1)}, u32[]{:S(2)}) copy-start(bf16[256,256]{1,0:T(8,128)(2,1)} %param.20) | copy-start | bytes 393220
  16.3 27.9 %collective-permute-start = (bf16[1024,256]{1,0:T(8,128)(2,1)S(1)}, bf16[1024,256]{1,0:T(8,128)(2,1)S(1)}, u32[]{:S(2)}, u32[]{:S(2)}) collective-permute-start(bf16[1024,256]{1,0:T(8,128)(2,1)S(1)} %get-tuple-element.7), channel_id=1, source_target_pairs={{0,120},{8,112},{16,104},{24,96},{32,88},{40,80},{48,72},{56,64},{... | collective-permute-start | bytes 1572872 | tf_op jit(solution)/shard_map/ppermute | solution.py:203
  44.4 1.6 copy-start
  100.7 60.0 %copy-start.1 = (bf16[128,2048]{1,0:T(8,128)(2,1)S(1)}, bf16[128,2048]{1,0:T(8,128)(2,1)}, u32[]{:S(2)}) copy-start(bf16[128,2048]{1,0:T(8,128)(2,1)} %param.13) | copy-start | bytes 1572868
  160.7 4.8 %copy-start.9 = (f32[2048]{0:T(1024)S(1)}, f32[2048]{0:T(1024)}, u32[]{:S(2)}) copy-start(f32[2048]{0:T(1024)} %param.22) | copy-start | bytes 24580
  166.5 161.6 %reduce-scatter.2.cloned.1.call-start = ((), (), s32[]{:S(2)}) async-start(), calls=%async_computation.5 | async-start | bytes 4718592 | tf_op jit(solution)/shard_map/reduce_scatter | solution.py:240
Sparse Core Ops, SparseCore 0:
  11.9 88.7 all-gather.11
  102.4 49.1 all-gather.5
  153.7 83.4 all-gather.9
  238.8 31.2 all-gather.7
  290.1 37.8 reduce-scatter.1
